TPU v7x, 256 devices: a whole 4x4x8 slice. The times are simulated.
256 devices in a mesh: sp: 16 (over y, x), tp: 16 (over z, core).
Axes of the slice: x: 4, y: 4, z: 8, core: 2. Of those that a mesh axis runs over, the one named last changes fastest.
Arguments:
- conv_value: bfloat16 [1024, 16384], P('tp', 'sp'), may hold values from -6 to 6
- conv_gate: bfloat16 [1024, 16384], P('tp', 'sp'), may hold values from -6 to 6
- conv_taps: float32 [1024, 31], P('tp'), may hold values from -2.2 to 2.2
- norm_gain: float32 [1024], replicated, may hold values from 0.1 to 1.9
- norm_bias: float32 [1024], replicated, may hold values from -3 to 3
- out_weight: bfloat16 [1024, 2048], replicated, may hold values from -0.1875 to 0.1875
- stream: bfloat16 [16384, 2048], P(('sp', 'tp')), may hold values from -6 to 6
- routes: int32 [16384, 2], P(('sp', 'tp')), may hold values from 0 to 15, all different within a row; in each aligned block of 64 rows (0 to 63, 64 to 127, ...) at most 8 rows name the same one
- route_weights: float32 [16384, 2], P(('sp', 'tp')), may hold values from 0.2 to 1
- expert_gain: float32 [2048], replicated, may hold values from 0.1 to 1.9
- expert_gate: bfloat16 [16, 2048, 7168], P('sp', None, 'tp'), may hold values from -0.125 to 0.125
- expert_up: bfloat16 [16, 2048, 7168], P('sp', None, 'tp'), may hold values from -0.125 to 0.125
- expert_down: bfloat16 [16, 7168, 2048], P('sp', 'tp'), may hold values from -0.0625 to 0.0625
Outputs:
- mixed: bfloat16 [16384, 2048], P(('sp', 'tp'))
Inputs may be any that keep to these rules, and one draw needn't show every extreme that they name: `routes`: within each device's 64 rows every expert is named exactly 8 times; a row names distinct experts.
All inputs are finite; a program needn't handle non-finite values.
Results may differ from a plain program's by a relative error of at most 0.014.
Values may be sent and summed in bfloat16 or wider, within the bound.
A program may use at most 64 MiB of HBM per device.

v0:
```python
import jax
import jax.numpy as jnp
from jax import lax
from jax.sharding import PartitionSpec as P

epsilon = 1e-06


def shifted(value, axis, steps):
    count = lax.axis_size(axis)
    initial, last = (max(0, -steps), min(count, count - steps))
    return lax.ppermute(value, axis, [(source, source + steps) for source in range(initial, last)])


def per_device(
    conv_value,
    conv_gate,
    conv_taps,
    norm_gain,
    norm_bias,
    out_weight,
    stream,
    routes,
    route_weights,
    expert_gain,
    expert_gate,
    expert_up,
    expert_down,
):
    f32 = jnp.float32
    local_ch = conv_value.shape[0]
    run_len = conv_value.shape[1]
    kernel_len = conv_taps.shape[1]
    gated_input = (conv_value.astype(f32) * jax.nn.sigmoid(conv_gate.astype(f32))).astype(
        jnp.bfloat16
    )
    left_rim = shifted(gated_input[:, run_len - (kernel_len - 1) :], "sp", 1)
    padded = jnp.concatenate([left_rim, gated_input], axis=1).astype(f32)
    conv_sum = jnp.zeros((local_ch, run_len), f32)
    for offset in range(kernel_len):
        conv_sum = (
            conv_sum + conv_taps[:, offset : offset + 1] * padded[:, offset : offset + run_len]
        )
    conv_out = conv_sum.astype(jnp.bfloat16)
    whole_conv = lax.all_to_all(conv_out, "tp", split_axis=1, concat_axis=0, tiled=True).astype(f32)
    center = jnp.mean(whole_conv, axis=0, keepdims=True)
    spread = jnp.mean((whole_conv - center) ** 2, axis=0, keepdims=True)
    scaled = (whole_conv - center) * lax.rsqrt(spread + epsilon) * norm_gain[:, None] + norm_bias[
        :, None
    ]
    token_major = jax.nn.silu(scaled).astype(jnp.bfloat16)
    projected = lax.dot_general(
        token_major, out_weight, (((0,), (0,)), ((), ())), preferred_element_type=f32
    )
    residual = (stream.astype(f32) + projected).astype(jnp.bfloat16)
    res_float = residual.astype(f32)
    normed = (
        res_float
        * lax.rsqrt(jnp.mean(res_float * res_float, axis=1, keepdims=True) + epsilon)
        * expert_gain
    ).astype(jnp.bfloat16)
    tok_rows = stream.shape[0]
    width = stream.shape[1]
    top_count = routes.shape[1]
    experts = lax.axis_size("sp")
    capacity = top_count * tok_rows // experts
    flat_ids = routes.reshape(-1)
    onehot = (flat_ids[:, None] == jnp.arange(experts, dtype=jnp.int32)[None, :]).astype(jnp.int32)
    before = jnp.cumsum(onehot, axis=0) - onehot
    rank = jnp.sum(before * onehot, axis=1)
    slots = flat_ids * capacity + rank
    chooser = jnp.any(
        slots.reshape(tok_rows, top_count)[None, :, :]
        == jnp.arange(experts * capacity, dtype=jnp.int32)[:, None, None],
        axis=2,
    ).astype(jnp.bfloat16)
    send_rows = (
        jnp.dot(chooser, normed, preferred_element_type=f32)
        .astype(jnp.bfloat16)
        .reshape(experts, capacity, width)
    )
    gate_w = expert_gate[0]
    up_w = expert_up[0]
    down_w = expert_down[0]
    received = lax.all_to_all(send_rows, "sp", split_axis=0, concat_axis=0, tiled=True)
    flat_recv = received.reshape(-1, width)
    piece = lax.all_gather(flat_recv, "tp", axis=0, tiled=True)
    gate_val = jnp.dot(piece, gate_w, preferred_element_type=f32)
    up_val = jnp.dot(piece, up_w, preferred_element_type=f32)
    hidden = (jax.nn.silu(gate_val) * up_val).astype(jnp.bfloat16)
    summed = lax.psum_scatter(
        jnp.dot(hidden, down_w, preferred_element_type=f32).astype(jnp.bfloat16),
        "tp",
        scatter_dimension=0,
        tiled=True,
    )
    result = summed.reshape(received.shape)
    returned = lax.all_to_all(result, "sp", split_axis=0, concat_axis=0, tiled=True)
    picked = returned.reshape(experts * capacity, width)[slots].reshape(tok_rows, top_count, width)
    expert_sum = jnp.sum(picked.astype(f32) * route_weights[:, :, None], axis=1)
    return (res_float + expert_sum).astype(jnp.bfloat16)


def solution(mesh):
    return jax.shard_map(
        per_device,
        mesh=mesh,
        in_specs=(
            P("tp", "sp"),
            P("tp", "sp"),
            P("tp", None),
            P(),
            P(),
            P(),
            P(("sp", "tp"), None),
            P(("sp", "tp"), None),
            P(("sp", "tp"), None),
            P(),
            P("sp", None, "tp"),
            P("sp", None, "tp"),
            P("sp", "tp", None),
        ),
        out_specs=P(("sp", "tp"), None),
        check_vma=False,
    )
```

profile of v0, /device:TPU:2, one launch (start us, length us, event | category | flops | bytes accessed | tf_op | source)
XLA Modules:
  0.0 225.3 jit_solution(4182957621673231946)
XLA Ops:
  6.5 1.2 multiply_convert_fusion.4
  7.8 3.4 %collective-permute-start = (bf16[64,30]{1,0:T(8,128)(2,1)S(1)}, bf16[64,30]{1,0:T(8,128)(2,1)S(1)}, u32[]{:S(2)}, u32[]{:S(2)}) collective-permute-start(bf16[64,30]{1,0:T(8,128)(2,1)S(1)} %slice.254), channel_id=1, source_target_pairs={{0,16},{16,32},{32,48},{48,64},{64,80},{80,96},{96,112},{112,128},... | collective-permute-start | bytes 11528 | tf_op jit(solution)/shard_map/ppermute | solution.py:12
  11.2 1.0 slice_bitcast_fusion.30
  12.2 1.0 slice_bitcast_fusion.29
  13.2 0.8 copy.28
  14.2 0.2 reduce_window_sum.11
  14.4 0.2 select_reduce_fusion
  14.8 2.7 %fusion.10 = bf16[64,1024]{1,0:T(8,128)(2,1)S(1)} fusion(f32[64,1054]{1,0:T(8,128)S(1)} %maximum_convert_fusion, f32[64]{0:T(128)S(1)} %get-tuple-element.36, f32[64]{0:T(128)S(1)} %get-tuple-element.37, f32[64]{0:T(128)S(1)} %get-tuple-element.8, f32[64]{0:T(128)S(1)} %get-tuple-element.9, f32[64]{0:T(128)S(1)} %get-tuple-element.10, ...), kind=kLoop, calls=%fused_computation.23 | loop fusion | flops 4063232 | bytes 8265472 | tf_op jit(solution)/shard_map/convert_element_type | solution.py:44
  17.5 0.2 copy.26
  17.7 0.9 reshape.99
  18.6 8.6 %all-to-all-start = ((bf16[16,2,2048]{2,1,0:T(2,128)(2,1)}), bf16[16,2,2048]{2,1,0:T(2,128)(2,1)S(1)}, u32[]{:S(2)}, u32[]{:S(2)}) async-start(bf16[16,2,2048]{2,1,0:T(2,128)(2,1)} %reshape.99), calls=%async_computation | async-start | bytes 262144 | tf_op jit(solution)/shard_map/all_to_all | solution.py:45
  27.4 8.4 %all-to-all-done = bf16[16,2,2048]{2,1,0:T(2,128)(2,1)S(1)} async-done(((bf16[16,2,2048]{2,1,0:T(2,128)(2,1)}), bf16[16,2,2048]{2,1,0:T(2,128)(2,1)S(1)}, u32[]{:S(2)}, u32[]{:S(2)}) %all-to-all-start) | async-done | bytes 131104 | tf_op jit(solution)/shard_map/all_to_all | solution.py:45
  35.8 0.2 reshape.100
  36.1 0.2 convert_reduce_fusion
  36.3 0.3 copy.27
  36.6 0.2 reshape.89
  36.8 0.3 fusion.8
  37.1 3.3 %multiply_reduce_fusion.1 = (f32[64]{0:T(128)S(1)}, f32[64,2048]{1,0:T(8,128)S(1)}) fusion(bf16[1024,2048]{1,0:T(8,128)(2,1)} %param.18, f32[1024,64]{0,1:T(8,128)S(1)} %reshape.89, f32[1024]{0:T(1024)S(1)} %copy-done.3, f32[1024]{0:T(1024)S(1)} %copy-done.4, f32[64]{0:T(128)S(1)} %add_rsqrt_fusion.1, f32[64]{0:T(128)S(1)} %broadcast_multiply_fusion.1, ...), kind=kOutput, calls=%fused_computation.20 | convolution fusion | flops 269811648 | bytes 5251840 | tf_op jit(solution)/shard_map/dot_general | solution.py:52
  40.4 0.4 fusion
  40.7 18.1 %all_to_all.23 = bf16[16,8,2048]{2,1,0:T(8,128)(2,1)} all-to-all(bf16[16,8,2048]{2,1,0:T(8,128)(2,1)S(1)} %fusion), channel_id=1, replica_groups=mesh['sp'=16,'tp'=16] {'sp'}, dimensions={0} | all-to-all | bytes 1048576 | tf_op jit(solution)/shard_map/all_to_all | solution.py:85
  58.8 0.2 reduce-scatter.2.cloned.1.call-start
  59.1 49.8 %all-gather.2.cloned.1.call-done = bf16[2048,2048]{1,0:T(8,128)(2,1)} async-done(((bf16[128,2048]{1,0:T(8,128)(2,1)}), bf16[2048,2048]{1,0:T(8,128)(2,1)}) %all-gather.2.cloned.1.call-update) | async-done | bytes 8388624 | tf_op jit(solution)/shard_map/all_gather | solution.py:87
  108.8 7.2 %fusion.5 = f32[2048,448]{0,1:T(8,128)S(1)} fusion(bf16[2048,2048]{1,0:T(8,128)(2,1)} %all-gather.2.cloned.1.call-done, bf16[1,2048,448]{1,2,0:T(8,128)(2,1)} %param.23), kind=kOutput, calls=%fused_computation.10 | convolution fusion | flops 3758096384 | bytes 13893632 | tf_op jit(solution)/shard_map/dot_general | solution.py:88
  116.0 4.3 %multiply_convert_fusion = bf16[2048,448]{0,1:T(8,128)(2,1)S(1)} fusion(f32[2048,448]{0,1:T(8,128)S(1)} %fusion.5, bf16[2048,2048]{1,0:T(8,128)(2,1)S(1)} %copy-done.6, bf16[1,2048,448]{1,2,0:T(8,128)(2,1)S(1)} %copy-done.7), kind=kOutput, calls=%fused_computation.2 | convolution fusion | flops 3763601408 | bytes 15728640 | tf_op jit(solution)/shard_map/dot_general | solution.py:89
  120.3 6.9 %convolution_convert_fusion = bf16[2048,2048]{1,0:T(8,128)(2,1)} fusion(bf16[2048,448]{0,1:T(8,128)(2,1)S(1)} %multiply_convert_fusion, bf16[1,448,2048]{2,1,0:T(8,128)(2,1)S(1)} %copy-done), kind=kOutput, calls=%fused_computation.1 | convolution fusion | flops 3762290688 | bytes 12058624 | tf_op jit(solution)/shard_map/dot_general | solution.py:92
  127.2 69.5 %reduce-scatter.2.cloned.1.call-done = bf16[128,2048]{1,0:T(8,128)(2,1)} async-done(((bf16[2048,2048]{1,0:T(8,128)(2,1)}), bf16[128,2048]{1,0:T(8,128)(2,1)}) %reduce-scatter.2.cloned.1.call-update) | async-done | bytes 524304 | tf_op jit(solution)/shard_map/reduce_scatter | solution.py:91
  196.8 7.1 %all-to-all-start.2 = ((bf16[16,8,2048]{2,1,0:T(8,128)(2,1)}), bf16[16,8,2048]{2,1,0:T(8,128)(2,1)S(1)}, u32[]{:S(2)}, u32[]{:S(2)}) async-start(bf16[16,8,2048]{2,1,0:T(8,128)(2,1)} %bitcast.100), calls=%async_computation.3 | async-start | bytes 1048576 | tf_op jit(solution)/shard_map/all_to_all | solution.py:98
  204.2 8.5 %all-to-all-done.2 = bf16[16,8,2048]{2,1,0:T(8,128)(2,1)S(1)} async-done(((bf16[16,8,2048]{2,1,0:T(8,128)(2,1)}), bf16[16,8,2048]{2,1,0:T(8,128)(2,1)S(1)}, u32[]{:S(2)}, u32[]{:S(2)}) %all-to-all-start.2) | async-done | bytes 524320 | tf_op jit(solution)/shard_map/all_to_all | solution.py:98
  212.7 1.7 gather_fusion
  214.4 1.7 reshape.90
  216.1 1.6 multiply_reduce_fusion
  217.7 0.8 add_convert_fusion
  (36 shorter events, 1.1 us)
Async XLA Ops:
  6.5 113.8 %copy-start = (bf16[1,448,2048]{2,1,0:T(8,128)(2,1)S(1)}, bf16[1,448,2048]{2,1,0:T(8,128)(2,1)}, u32[]{:S(2)}) copy-start(bf16[1,448,2048]{2,1,0:T(8,128)(2,1)} %param.25) | copy-start | bytes 5505028
  7.8 6.9 %collective-permute-start = (bf16[64,30]{1,0:T(8,128)(2,1)S(1)}, bf16[64,30]{1,0:T(8,128)(2,1)S(1)}, u32[]{:S(2)}, u32[]{:S(2)}) collective-permute-start(bf16[64,30]{1,0:T(8,128)(2,1)S(1)} %slice.254), channel_id=1, source_target_pairs={{0,16},{16,32},{32,48},{48,64},{64,80},{80,96},{96,112},{112,128},... | collective-permute-start | bytes 11528 | tf_op jit(solution)/shard_map/ppermute | solution.py:12
  17.5 19.5 %copy-start.1 = (bf16[64,2048]{1,0:T(8,128)(2,1)S(1)}, bf16[64,2048]{1,0:T(8,128)(2,1)}, u32[]{:S(2)}) copy-start(bf16[64,2048]{1,0:T(8,128)(2,1)} %param.19) | copy-start | bytes 786436
  17.5 19.5 %copy-start.3 = (f32[1024]{0:T(1024)S(1)}, f32[1024]{0:T(1024)}, u32[]{:S(2)}) copy-start(f32[1024]{0:T(1024)} %param.17) | copy-start | bytes 12292
  17.5 19.5 %copy-start.4 = (f32[1024]{0:T(1024)S(1)}, f32[1024]{0:T(1024)}, u32[]{:S(2)}) copy-start(f32[1024]{0:T(1024)} %param.16) | copy-start | bytes 12292
  18.6 17.2 %all-to-all-start = ((bf16[16,2,2048]{2,1,0:T(2,128)(2,1)}), bf16[16,2,2048]{2,1,0:T(2,128)(2,1)S(1)}, u32[]{:S(2)}, u32[]{:S(2)}) async-start(bf16[16,2,2048]{2,1,0:T(2,128)(2,1)} %reshape.99), calls=%async_computation | async-start | bytes 262144 | tf_op jit(solution)/shard_map/all_to_all | solution.py:45
  27.2 81.6 %all-gather.2.cloned.1.call-start = ((), (), s32[]{:S(2)}) async-start(), calls=%async_computation.4 | async-start | bytes 8912896 | tf_op jit(solution)/shard_map/all_gather | solution.py:87
  36.3 4.1 %copy-start.2 = (f32[2048]{0:T(1024)S(1)}, f32[2048]{0:T(1024)}, u32[]{:S(2)}) copy-start(f32[2048]{0:T(1024)} %param.22) | copy-start | bytes 24580
  58.8 138.0 %reduce-scatter.2.cloned.1.call-start = ((), (), s32[]{:S(2)}) async-start(), calls=%async_computation.5 | async-start | bytes 8912896 | tf_op jit(solution)/shard_map/reduce_scatter | solution.py:91
  108.8 7.2 %copy-start.6 = (bf16[2048,2048]{1,0:T(8,128)(2,1)S(1)}, bf16[2048,2048]{1,0:T(8,128)(2,1)}, u32[]{:S(2)}) copy-start(bf16[2048,2048]{1,0:T(8,128)(2,1)} %all-gather.2.cloned.1.call-done) | copy-start | bytes 25165828
  108.8 7.2 %copy-start.7 = (bf16[1,2048,448]{1,2,0:T(8,128)(2,1)S(1)}, bf16[1,2048,448]{1,2,0:T(8,128)(2,1)}, u32[]{:S(2)}) copy-start(bf16[1,2048,448]{1,2,0:T(8,128)(2,1)} %param.24) | copy-start | bytes 5505028
  127.2 76.8 %copy-start.5 = (f32[64,2]{0,1:T(2,128)S(1)}, f32[64,2]{0,1:T(2,128)}, u32[]{:S(2)}) copy-start(f32[64,2]{0,1:T(2,128)} %param.21) | copy-start | bytes 1540
  196.8 15.9 %all-to-all-start.2 = ((bf16[16,8,2048]{2,1,0:T(8,128)(2,1)}), bf16[16,8,2048]{2,1,0:T(8,128)(2,1)S(1)}, u32[]{:S(2)}, u32[]{:S(2)}) async-start(bf16[16,8,2048]{2,1,0:T(8,128)(2,1)} %bitcast.100), calls=%async_computation.3 | async-start | bytes 1048576 | tf_op jit(solution)/shard_map/all_to_all | solution.py:98
Sparse Core Ops, SparseCore 0:
  59.0 49.8 all-gather.1
  127.4 69.3 reduce-scatter.1
where the time goes:
time: 226 us; the launch traced here: 225 us
  waiting for transfers between devices  136 us (60%)
  matrix products  22 us (10%)
  starting transfers between devices  19.3 us (9%)
  blocking collectives  18.1 us (8%)
  between operations  13.7 us (6%)
  local copies, waits for them, and re-layouts  8.64 us (4%)
  other arithmetic  7.29 us (3%)
    reduce_scatter x1, waiting for transfers between devices, per_device(): lax.psum_scatter(jnp.dot(hidden, down_w, preferred_element_type=f32).asty...  69.5 us
    all_gather x1, waiting for transfers between devices, per_device(): piece = lax.all_gather(flat_recv, 'tp', axis=0, tiled=True)  49.8 us
    all_to_all x1, blocking collectives, per_device(): lax.all_to_all(send_rows, 'sp', split_axis=0, concat_axis=0, tiled=True)  18.1 us
    all_to_all x1, starting transfers between devices, per_device(): lax.all_to_all(conv_out, 'tp', split_axis=1, concat_axis=0, tiled=True)  8.57 us
    all_to_all x1, waiting for transfers between devices, per_device(): lax.all_to_all(result, 'sp', split_axis=0, concat_axis=0, tiled=True)  8.52 us
    all_to_all x1, waiting for transfers between devices, per_device(): lax.all_to_all(conv_out, 'tp', split_axis=1, concat_axis=0, tiled=True)  8.41 us
    dot_general x1, matrix products, per_device(): gate_val = jnp.dot(piece, gate_w, preferred_element_type=f32)  7.17 us
    all_to_all x1, starting transfers between devices, per_device(): lax.all_to_all(result, 'sp', split_axis=0, concat_axis=0, tiled=True)  7.1 us
  transfers between devices with their start and end apart: 5, of which 4 were waited for; matrix products, arithmetic and copies ran while one was open for 2% of the time, Pallas kernels for 0%

commit v1 on v0

--- a/solution.py
+++ b/solution.py
@@ -84,7 +84,9 @@
     down_w = expert_down[0]
     received = lax.all_to_all(send_rows, "sp", split_axis=0, concat_axis=0, tiled=True)
     flat_recv = received.reshape(-1, width)
-    piece = lax.all_gather(flat_recv, "tp", axis=0, tiled=True)
+    piece = jnp.concatenate(
+        lax.all_to_all(jnp.stack([flat_recv] * lax.axis_size("tp")), "tp", 0, 0), axis=0
+    )
     gate_val = jnp.dot(piece, gate_w, preferred_element_type=f32)
     up_val = jnp.dot(piece, up_w, preferred_element_type=f32)
     hidden = (jax.nn.silu(gate_val) * up_val).astype(jnp.bfloat16)

time: 226 us -> 358 us (1.58)
  blocking collectives: 18.1 us -> 205 us
  waiting for transfers between devices: 136 us -> 83.6 us
    all_to_all x0 -> x1, blocking collectives: none -> 187 us  [per_device(): lax.all_to_all(jnp.stack([flat_recv] * lax.axis_size('tp')), 'tp', 0, 0)]
    all_gather x1 -> x0, waiting for transfers between devices: 49.8 us -> none  [per_device(): piece = lax.all_gather(flat_recv, 'tp', axis=0, tiled=True)]
  transfers between devices with their start and end apart: 5 -> 4, of which waited for: 4 -> 3; matrix products, arithmetic and copies ran while one was open for 2% -> 1% of each run, Pallas kernels for 0% -> 0%
where the time goes in v1:
time: 358 us; the launch traced here: 357 us
  blocking collectives  205 us (57%)
  waiting for transfers between devices  83.6 us (23%)
  starting transfers between devices  19.1 us (5%)
  matrix products  18.8 us (5%)
  between operations  13.7 us (4%)
  local copies, waits for them, and re-layouts  9.7 us (3%)
  other arithmetic  7.27 us (2%)
    all_to_all x1, blocking collectives, per_device(): lax.all_to_all(jnp.stack([flat_recv] * lax.axis_size('tp')), 'tp', 0, 0)  187 us
    reduce_scatter x1, waiting for transfers between devices, per_device(): lax.psum_scatter(jnp.dot(hidden, down_w, preferred_element_type=f32).asty...  66.7 us
    all_to_all x1, blocking collectives, per_device(): lax.all_to_all(send_rows, 'sp', split_axis=0, concat_axis=0, tiled=True)  18 us
    all_to_all x1, starting transfers between devices, per_device(): lax.all_to_all(conv_out, 'tp', split_axis=1, concat_axis=0, tiled=True)  8.57 us
    all_to_all x1, waiting for transfers between devices, per_device(): lax.all_to_all(result, 'sp', split_axis=0, concat_axis=0, tiled=True)  8.52 us
    all_to_all x1, waiting for transfers between devices, per_device(): lax.all_to_all(conv_out, 'tp', split_axis=1, concat_axis=0, tiled=True)  8.41 us
  transfers between devices with their start and end apart: 4, of which 3 were waited for; matrix products, arithmetic and copies ran while one was open for 1% of the time, Pallas kernels for 0%

profile of v1, /device:TPU:2, one launch (start us, length us, event | category | flops | bytes accessed | tf_op | source)
XLA Modules:
  0.0 357.4 jit_solution(16689211710930129502)
XLA Ops:
  6.5 1.2 multiply_convert_fusion.4
  7.8 3.4 collective-permute-start
  11.2 1.0 slice_bitcast_fusion.30
  12.2 1.0 slice_bitcast_fusion.29
  13.2 0.8 copy.28
  14.2 0.2 reduce_window_sum.11
  14.4 0.2 select_reduce_fusion
  14.8 2.7 fusion.10
  17.5 0.2 copy.26
  17.7 0.9 reshape.101
  18.6 8.6 %all-to-all-start = ((bf16[16,2,2048]{2,1,0:T(2,128)(2,1)}), bf16[16,2,2048]{2,1,0:T(2,128)(2,1)S(1)}, u32[]{:S(2)}, u32[]{:S(2)}) async-start(bf16[16,2,2048]{2,1,0:T(2,128)(2,1)} %reshape.101), calls=%async_computation | async-start | bytes 262144 | tf_op jit(solution)/shard_map/all_to_all | solution.py:45
  27.4 8.4 %all-to-all-done = bf16[16,2,2048]{2,1,0:T(2,128)(2,1)S(1)} async-done(((bf16[16,2,2048]{2,1,0:T(2,128)(2,1)}), bf16[16,2,2048]{2,1,0:T(2,128)(2,1)S(1)}, u32[]{:S(2)}, u32[]{:S(2)}) %all-to-all-start) | async-done | bytes 131104 | tf_op jit(solution)/shard_map/all_to_all | solution.py:45
  35.8 0.2 reshape.102
  36.1 0.2 convert_reduce_fusion
  36.3 0.3 copy.27
  36.6 0.2 reshape.91
  36.8 0.3 fusion.8
  37.1 3.3 multiply_reduce_fusion.1
  40.4 0.4 fusion
  40.7 18.0 %all_to_all.28 = bf16[16,8,2048]{2,1,0:T(8,128)(2,1)S(1)} all-to-all(bf16[16,8,2048]{2,1,0:T(8,128)(2,1)S(1)} %fusion), channel_id=1, replica_groups=mesh['sp'=16,'tp'=16] {'sp'}, dimensions={0} | all-to-all | bytes 1048576 | tf_op jit(solution)/shard_map/all_to_all | solution.py:85
  58.7 1.1 stack.3
  59.8 187.3 %all_to_all.29 = bf16[16,128,2048]{2,1,0:T(8,128)(2,1)S(1)} all-to-all(bf16[16,128,2048]{2,1,0:T(8,128)(2,1)S(1)} %stack.3), channel_id=1, replica_groups=mesh['sp'=16,'tp'=16] {'tp'}, dimensions={0} | all-to-all | bytes 16777216 | tf_op jit(solution)/shard_map/all_to_all | solution.py:88
  247.0 4.0 %fusion.5 = f32[2048,448]{0,1:T(8,128)S(1)} fusion(bf16[2048,2048]{1,0:T(8,128)(2,1)S(1)} %bitcast.99, bf16[1,2048,448]{1,2,0:T(8,128)(2,1)S(1)} %copy-done.6), kind=kOutput, calls=%fused_computation.10 | convolution fusion | flops 3758096384 | bytes 13893632 | tf_op jit(solution)/shard_map/dot_general | solution.py:90
  251.1 4.3 %multiply_convert_fusion = bf16[2048,448]{0,1:T(8,128)(2,1)S(1)} fusion(f32[2048,448]{0,1:T(8,128)S(1)} %fusion.5, bf16[2048,2048]{1,0:T(8,128)(2,1)S(1)} %bitcast.100, bf16[1,2048,448]{1,2,0:T(8,128)(2,1)S(1)} %copy-done.7), kind=kOutput, calls=%fused_computation.2 | convolution fusion | flops 3763601408 | bytes 15728640 | tf_op jit(solution)/shard_map/dot_general | solution.py:91
  255.4 6.9 %convolution_convert_fusion = bf16[2048,2048]{1,0:T(8,128)(2,1)} fusion(bf16[2048,448]{0,1:T(8,128)(2,1)S(1)} %multiply_convert_fusion, bf16[1,448,2048]{2,1,0:T(8,128)(2,1)S(1)} %copy-done), kind=kOutput, calls=%fused_computation.1 | convolution fusion | flops 3762290688 | bytes 12058624 | tf_op jit(solution)/shard_map/dot_general | solution.py:94
  262.3 66.7 %reduce-scatter.2.cloned.1.call-done = bf16[128,2048]{1,0:T(8,128)(2,1)} async-done(((bf16[2048,2048]{1,0:T(8,128)(2,1)}), bf16[128,2048]{1,0:T(8,128)(2,1)}) %reduce-scatter.2.cloned.1.call-update) | async-done | bytes 524304 | tf_op jit(solution)/shard_map/reduce_scatter | solution.py:93
  329.0 7.1 %all-to-all-start.3 = ((bf16[16,8,2048]{2,1,0:T(8,128)(2,1)}), bf16[16,8,2048]{2,1,0:T(8,128)(2,1)S(1)}, u32[]{:S(2)}, u32[]{:S(2)}) async-start(bf16[16,8,2048]{2,1,0:T(8,128)(2,1)} %bitcast.103), calls=%async_computation.4 | async-start | bytes 1048576 | tf_op jit(solution)/shard_map/all_to_all | solution.py:100
  336.3 8.5 %all-to-all-done.3 = bf16[16,8,2048]{2,1,0:T(8,128)(2,1)S(1)} async-done(((bf16[16,8,2048]{2,1,0:T(8,128)(2,1)}), bf16[16,8,2048]{2,1,0:T(8,128)(2,1)S(1)}, u32[]{:S(2)}, u32[]{:S(2)}) %all-to-all-start.3) | async-done | bytes 524320 | tf_op jit(solution)/shard_map/all_to_all | solution.py:100
  344.8 1.7 gather_fusion
  346.6 1.7 reshape.92
  348.3 1.5 multiply_reduce_fusion
  349.8 0.8 add_convert_fusion
  (35 shorter events, 1.1 us)
Async XLA Ops:
  6.5 248.9 %copy-start = (bf16[1,448,2048]{2,1,0:T(8,128)(2,1)S(1)}, bf16[1,448,2048]{2,1,0:T(8,128)(2,1)}, u32[]{:S(2)}) copy-start(bf16[1,448,2048]{2,1,0:T(8,128)(2,1)} %param.25) | copy-start | bytes 5505028
  7.8 6.9 %collective-permute-start = (bf16[64,30]{1,0:T(8,128)(2,1)S(1)}, bf16[64,30]{1,0:T(8,128)(2,1)S(1)}, u32[]{:S(2)}, u32[]{:S(2)}) collective-permute-start(bf16[64,30]{1,0:T(8,128)(2,1)S(1)} %slice.254), channel_id=1, source_target_pairs={{0,16},{16,32},{32,48},{48,64},{64,80},{80,96},{96,112},{112,128},... | collective-permute-start | bytes 11528 | tf_op jit(solution)/shard_map/ppermute | solution.py:12
  17.5 19.5 %copy-start.1 = (bf16[64,2048]{1,0:T(8,128)(2,1)S(1)}, bf16[64,2048]{1,0:T(8,128)(2,1)}, u32[]{:S(2)}) copy-start(bf16[64,2048]{1,0:T(8,128)(2,1)} %param.19) | copy-start | bytes 786436
  17.5 19.5 %copy-start.3 = (f32[1024]{0:T(1024)S(1)}, f32[1024]{0:T(1024)}, u32[]{:S(2)}) copy-start(f32[1024]{0:T(1024)} %param.17) | copy-start | bytes 12292
  17.5 19.5 %copy-start.4 = (f32[1024]{0:T(1024)S(1)}, f32[1024]{0:T(1024)}, u32[]{:S(2)}) copy-start(f32[1024]{0:T(1024)} %param.16) | copy-start | bytes 12292
  18.6 17.2 %all-to-all-start = ((bf16[16,2,2048]{2,1,0:T(2,128)(2,1)}), bf16[16,2,2048]{2,1,0:T(2,128)(2,1)S(1)}, u32[]{:S(2)}, u32[]{:S(2)}) async-start(bf16[16,2,2048]{2,1,0:T(2,128)(2,1)} %reshape.101), calls=%async_computation | async-start | bytes 262144 | tf_op jit(solution)/shard_map/all_to_all | solution.py:45
  27.2 301.8 %reduce-scatter.2.cloned.1.call-start = ((), (), s32[]{:S(2)}) async-start(), calls=%async_computation.5 | async-start | bytes 8912896 | tf_op jit(solution)/shard_map/reduce_scatter | solution.py:93
  36.3 4.1 %copy-start.2 = (f32[2048]{0:T(1024)S(1)}, f32[2048]{0:T(1024)}, u32[]{:S(2)}) copy-start(f32[2048]{0:T(1024)} %param.22) | copy-start | bytes 24580
  59.8 187.3 %copy-start.6 = (bf16[1,2048,448]{1,2,0:T(8,128)(2,1)S(1)}, bf16[1,2048,448]{1,2,0:T(8,128)(2,1)}, u32[]{:S(2)}) copy-start(bf16[1,2048,448]{1,2,0:T(8,128)(2,1)} %param.23) | copy-start | bytes 5505028
  247.0 4.0 %copy-start.7 = (bf16[1,2048,448]{1,2,0:T(8,128)(2,1)S(1)}, bf16[1,2048,448]{1,2,0:T(8,128)(2,1)}, u32[]{:S(2)}) copy-start(bf16[1,2048,448]{1,2,0:T(8,128)(2,1)} %param.24) | copy-start | bytes 5505028
  262.3 73.9 %copy-start.5 = (f32[64,2]{0,1:T(2,128)S(1)}, f32[64,2]{0,1:T(2,128)}, u32[]{:S(2)}) copy-start(f32[64,2]{0,1:T(2,128)} %param.21) | copy-start | bytes 1540
  329.0 15.9 %all-to-all-start.3 = ((bf16[16,8,2048]{2,1,0:T(8,128)(2,1)}), bf16[16,8,2048]{2,1,0:T(8,128)(2,1)S(1)}, u32[]{:S(2)}, u32[]{:S(2)}) async-start(bf16[16,8,2048]{2,1,0:T(8,128)(2,1)} %bitcast.103), calls=%async_computation.4 | async-start | bytes 1048576 | tf_op jit(solution)/shard_map/all_to_all | solution.py:100
Sparse Core Ops, SparseCore 0:
  262.4 66.4 reduce-scatter.1
